TPU v7x, 32 devices: a whole 2x2x4 slice. The times are simulated.
32 devices in a mesh: grp: 2 (over x), ep: 4 (over y, core), tp: 4 (over z).
Axes of the slice: x: 2, y: 2, z: 4, core: 2. Of those that a mesh axis runs over, the one named last changes fastest.
Arguments:
- tokens: bfloat16 [3072, 4096], P(('grp', 'ep'), 'tp'), parts along dimension 0
- pre_gain: float32 [4096], replicated, may hold values from 0.1 to 1.9
- out_gain: float32 [4096], P('tp'), may hold values from 0.1 to 1.9
- chosen: int32 [8, 4, 48], P(('grp', 'ep')), parts along dimension 0, may hold values from 0 to 383, as said below
- route_weight: float32 [8, 4, 48], P(('grp', 'ep')), parts along dimension 0, may hold values from 0.3 to 3
- expert_gate: bfloat16 [4, 4096, 3072], P('ep', None, 'tp'), may hold values from -0.09375 to 0.09375
- expert_up: bfloat16 [4, 4096, 3072], P('ep', None, 'tp'), may hold values from -0.09375 to 0.09375
- expert_down: bfloat16 [4, 3072, 4096], P('ep', 'tp'), may hold values from -0.109375 to 0.109375
Outputs:
- output: bfloat16 [3072, 4096], P(('grp', 'ep'), 'tp'), parts along dimension 0
There are 2 independent parts, one for each index of `grp`. A program takes and returns all parts, laid end to end along the dimension named above; an argument that names none is the same for every part. Nothing has to cross between parts.
Inputs may be any that keep to these rules, and one draw needn't show every extreme that they name: chosen[b, e, k] is the position, within block b of 384 tokens, of the k-th token that expert e takes from that block; the 48 positions of one block and one expert are all different.
All inputs are finite; a program needn't handle non-finite values.
Results may differ from a plain program's by a relative error of at most 0.0075.
Values may be sent and summed in bfloat16 or wider, within the bound.
No kernel may reach another device: no remote copies, remote signals or barrier semaphores. Data moves between devices by JAX's collectives and lax.ppermute only.
A program may use at most 64 MiB of HBM per device.

v0:
```python
import jax
import jax.numpy as jnp
from jax import lax
from jax.sharding import PartitionSpec as P

NORM_EPS = 1e-06


def shards(tokens, pre_gain, out_gain, chosen, route_weight, expert_gate, expert_up, expert_down):
    model_width = pre_gain.shape[0]
    shard_width = tokens.shape[1]
    tok_count = tokens.shape[0]
    chosen_here = chosen[0]
    experts_all = chosen_here.shape[0]
    slot_count = chosen_here.shape[1]
    resident = tokens.astype(jnp.float32)
    square_sum = lax.psum(jnp.sum(resident * resident, axis=1), "tp")
    row_scale = lax.rsqrt(square_sum / model_width + NORM_EPS)[:, None]
    gain_slice = lax.dynamic_slice_in_dim(
        pre_gain, lax.axis_index("tp") * shard_width, shard_width, 0
    )
    normed = (resident * row_scale * gain_slice).astype(jnp.bfloat16)
    outgoing = jnp.take(normed, chosen_here, axis=0)
    incoming = lax.all_to_all(outgoing, "ep", split_axis=0, concat_axis=0, tiled=True)
    picked_rows = lax.all_gather(incoming.reshape(-1, shard_width), "tp", axis=1, tiled=True)
    gate_act = jnp.dot(picked_rows, expert_gate[0], preferred_element_type=jnp.float32)
    up_act = jnp.dot(picked_rows, expert_up[0], preferred_element_type=jnp.float32)
    hidden = (jax.nn.silu(gate_act) * up_act).astype(jnp.bfloat16)
    down_shard = expert_down[0]
    summed = lax.psum_scatter(
        lax.dot_general(
            down_shard, hidden, (((0,), (1,)), ((), ())), preferred_element_type=jnp.float32
        ).astype(jnp.bfloat16),
        "tp",
        scatter_dimension=0,
        tiled=True,
    )
    expert_out = summed.reshape(shard_width, experts_all, slot_count)
    returned = lax.all_to_all(expert_out, "ep", split_axis=1, concat_axis=1, tiled=True)
    weighted = returned.astype(jnp.float32) * route_weight[0][None]
    flat_weighted = weighted.reshape(shard_width, experts_all * slot_count)
    update_cols = (
        jnp.zeros((shard_width, tok_count), jnp.float32)
        .at[:, chosen_here.reshape(-1)]
        .add(flat_weighted)
    )
    mixed_rows = resident + update_cols.T
    out_sum = lax.psum(jnp.sum(mixed_rows * mixed_rows, axis=1), "tp")
    out_scale = lax.rsqrt(out_sum / model_width + NORM_EPS)[:, None]
    return (mixed_rows * out_scale * out_gain).astype(jnp.bfloat16)


def solution(mesh):
    return jax.shard_map(
        shards,
        mesh=mesh,
        in_specs=(
            P(("grp", "ep"), "tp"),
            P(),
            P("tp"),
            P(("grp", "ep"), None, None),
            P(("grp", "ep"), None, None),
            P("ep", None, "tp"),
            P("ep", None, "tp"),
            P("ep", "tp", None),
        ),
        out_specs=P(("grp", "ep"), "tp"),
        check_vma=False,
    )
```

profile of v0, /device:TPU:0, one launch (start us, length us, event | category | flops | bytes accessed | tf_op | source)
XLA Modules:
  0.0 150.9 jit_solution(1247583569600255627)
XLA Ops:
  6.5 0.0 all-gather.2.cloned.1.call-start
  6.5 0.7 compare_select_fusion.1
  7.2 0.7 compare_and_fusion
  7.9 1.4 fusion.12
  9.3 13.5 %psum.14 = f32[384]{0:T(512)S(1)} all-reduce(f32[384]{0:T(512)S(1)} %fusion.12), channel_id=1, replica_groups=mesh['grp'=2,'ep'=4,'tp'=4] {'tp'}, use_global_device_ids=true, to_apply=%region_1.0 | all-reduce | flops 384 | bytes 3072 | tf_op jit(solution)/shard_map/psum | solution.py:17
  22.8 0.1 reshape.80
  22.9 0.7 dynamic_slice.3
  23.6 1.4 fusion.14
  24.9 1.0 gather_fusion
  26.0 0.1 broadcast_select_fusion
  26.1 10.5 %all_to_all.10 = bf16[4,48,1024]{2,1,0:T(8,128)(2,1)} all-to-all(bf16[4,48,1024]{2,1,0:T(8,128)(2,1)S(1)} %broadcast_select_fusion), channel_id=1, replica_groups=mesh['grp'=2,'ep'=4,'tp'=4] {'ep'}, dimensions={0} | all-to-all | bytes 786432 | tf_op jit(solution)/shard_map/all_to_all | solution.py:24
  36.5 0.0 all-gather.2.cloned.1.call-update
  36.6 0.0 reduce-scatter.2.cloned.1.call-start
  36.6 34.4 %all-gather.2.cloned.1.call-done = bf16[192,4096]{1,0:T(8,128)(2,1)} async-done(((bf16[192,1024]{1,0:T(8,128)(2,1)}), bf16[192,4096]{1,0:T(8,128)(2,1)}) %all-gather.2.cloned.1.call-update) | async-done | bytes 1572880 | tf_op jit(solution)/shard_map/all_gather | solution.py:25
  71.0 0.0 copy-start.4
  71.0 4.8 %fusion.4 = f32[192,768]{1,0:T(8,128)S(1)} fusion(bf16[192,4096]{1,0:T(8,128)(2,1)} %all-gather.2.cloned.1.call-done, bf16[1,4096,768]{2,1,0:T(8,128)(2,1)} %param.13), kind=kOutput, calls=%fused_computation.6 | convolution fusion | flops 1207959552 | bytes 8454144 | tf_op jit(solution)/shard_map/dot_general | solution.py:26
  75.8 0.0 copy-done.4
  75.8 9.3 %fusion.9 = bf16[4096,192]{0,1:T(8,128)(2,1)} fusion(bf16[1,768,4096]{2,1,0:T(8,128)(2,1)} %param.15, bf16[192,4096]{1,0:T(8,128)(2,1)S(1)} %copy-done.4, bf16[1,4096,768]{2,1,0:T(8,128)(2,1)} %param.14, f32[192,768]{1,0:T(8,128)S(1)} %fusion.4), kind=kOutput, calls=%fused_computation.9 | convolution fusion | flops 2417590272 | bytes 16318464 | tf_op jit(solution)/shard_map/dot_general | solution.py:31
  85.0 0.0 copy-start.1
  85.0 0.0 copy-start.3
  85.0 0.0 reduce-scatter.2.cloned.1.call-update
  85.1 34.4 %reduce-scatter.2.cloned.1.call-done = bf16[1024,192]{0,1:T(8,128)(2,1)} async-done(((bf16[4096,192]{0,1:T(8,128)(2,1)}), bf16[1024,192]{0,1:T(8,128)(2,1)}) %reduce-scatter.2.cloned.1.call-update) | async-done | bytes 393232 | tf_op jit(solution)/shard_map/reduce_scatter | solution.py:30
  119.5 3.5 %all-to-all-start.1 = ((bf16[1024,4,48]{0,2,1:T(8,128)(2,1)}), bf16[1024,4,48]{0,2,1:T(8,128)(2,1)S(1)}, u32[]{:S(2)}, u32[]{:S(2)}) async-start(bf16[1024,4,48]{0,2,1:T(8,128)(2,1)} %bitcast.48), calls=%async_computation.2 | async-start | bytes 786432 | tf_op jit(solution)/shard_map/all_to_all | solution.py:39
  123.0 0.0 copy-done.1
  123.0 0.0 copy-start
  123.0 0.1 reshape_squeeze.3
  123.1 7.3 %all-to-all-done.1 = bf16[1024,4,48]{0,2,1:T(8,128)(2,1)S(1)} async-done(((bf16[1024,4,48]{0,2,1:T(8,128)(2,1)}), bf16[1024,4,48]{0,2,1:T(8,128)(2,1)S(1)}, u32[]{:S(2)}, u32[]{:S(2)}) %all-to-all-start.1) | async-done | bytes 393248 | tf_op jit(solution)/shard_map/all_to_all | solution.py:39
  130.3 0.0 copy-done.3
  130.3 0.1 convert_multiply_fusion.2
  130.5 2.5 %scatter_custom_fusion = f32[1024,384]{0,1:T(8,128)S(1)} fusion(s32[192]{0:T(256)S(1)} %bitcast.50, f32[192,1024]{1,0:T(8,128)S(1)} %bitcast.47, f32[]{:T(128)} %constant.11.clone.1), kind=kCustom, calls=%fused_computation.21 | custom fusion | flops 196608 | bytes 1572868 | tf_op jit(solution)/shard_map/scatter-add | solution.py:45
  133.0 0.0 copy-done
  133.0 0.0 copy-start.2
  133.0 0.3 multiply_reduce_fusion
  133.3 9.6 %psum.15 = f32[384]{0:T(512)S(1)} all-reduce(f32[384]{0:T(512)S(1)} %multiply_reduce_fusion), channel_id=1, replica_groups=mesh['grp'=2,'ep'=4,'tp'=4] {'tp'}, use_global_device_ids=true, to_apply=%region_5.6 | all-reduce | flops 384 | bytes 3072 | tf_op jit(solution)/shard_map/psum | solution.py:48
  142.9 0.0 copy-done.2
  142.9 1.1 multiply_convert_fusion
  (4 shorter events, 0.0 us)
Async XLA Ops:
  6.5 64.5 %all-gather.2.cloned.1.call-start = ((), (), s32[]{:S(2)}) async-start(), calls=%async_computation.3 | async-start | bytes 1966080 | tf_op jit(solution)/shard_map/all_gather | solution.py:25
  36.6 82.9 %reduce-scatter.2.cloned.1.call-start = ((), (), s32[]{:S(2)}) async-start(), calls=%async_computation.4 | async-start | bytes 1966080 | tf_op jit(solution)/shard_map/reduce_scatter | solution.py:30
  71.0 4.8 %copy-start.4 = (bf16[192,4096]{1,0:T(8,128)(2,1)S(1)}, bf16[192,4096]{1,0:T(8,128)(2,1)}, u32[]{:S(2)}) copy-start(bf16[192,4096]{1,0:T(8,128)(2,1)} %all-gather.2.cloned.1.call-done) | copy-start | bytes 4718596
  85.0 37.9 %copy-start.1 = (s32[1,4,48]{2,1,0:T(4,128)S(1)}, s32[1,4,48]{2,1,0:T(4,128)}, u32[]{:S(2)}) copy-start(s32[1,4,48]{2,1,0:T(4,128)} %param.11) | copy-start | bytes 2308
  85.0 45.3 %copy-start.3 = (f32[1,4,48]{2,1,0:T(4,128)S(1)}, f32[1,4,48]{2,1,0:T(4,128)}, u32[]{:S(2)}) copy-start(f32[1,4,48]{2,1,0:T(4,128)} %param.12) | copy-start | bytes 2308
  119.5 10.8 %all-to-all-start.1 = ((bf16[1024,4,48]{0,2,1:T(8,128)(2,1)}), bf16[1024,4,48]{0,2,1:T(8,128)(2,1)S(1)}, u32[]{:S(2)}, u32[]{:S(2)}) async-start(bf16[1024,4,48]{0,2,1:T(8,128)(2,1)} %bitcast.48), calls=%async_computation.2 | async-start | bytes 786432 | tf_op jit(solution)/shard_map/all_to_all | solution.py:39
  123.0 10.0 %copy-start = (bf16[384,1024]{1,0:T(8,128)(2,1)S(1)}, bf16[384,1024]{1,0:T(8,128)(2,1)}, u32[]{:S(2)}) copy-start(bf16[384,1024]{1,0:T(8,128)(2,1)} %param.8) | copy-start | bytes 2359300
  133.0 9.9 %copy-start.2 = (f32[1024]{0:T(1024)S(1)}, f32[1024]{0:T(1024)}, u32[]{:S(2)}) copy-start(f32[1024]{0:T(1024)} %param.10) | copy-start | bytes 12292
Sparse Core Ops, SparseCore 0:
  36.7 34.2 all-gather.1
  85.2 34.2 reduce-scatter.1
where the time goes:
time: 151 us
  waiting for transfers between devices  76.1 us (50%)
  blocking collectives  33.6 us (22%)
  matrix products  14 us (9%)
  between operations  13.5 us (9%)
  other arithmetic  8.29 us (5%)
  starting transfers between devices  3.5 us (2%)
  local copies, waits for them, and re-layouts  1.9 us (1%)
    reduce_scatter x1, waiting for transfers between devices, shards(): lax.psum_scatter(lax.dot_general(down_shard, hidden, (((0,), (1,)), ((),...  34.4 us
    all_gather x1, waiting for transfers between devices, shards(): lax.all_gather(incoming.reshape(-1, shard_width), 'tp', axis=1, tiled=True)  34.4 us
    psum x1, blocking collectives, shards(): square_sum = lax.psum(jnp.sum(resident * resident, axis=1), 'tp')  13.5 us
    all_to_all x1, blocking collectives, shards(): lax.all_to_all(outgoing, 'ep', split_axis=0, concat_axis=0, tiled=True)  10.5 us
    psum x1, blocking collectives, shards(): out_sum = lax.psum(jnp.sum(mixed_rows * mixed_rows, axis=1), 'tp')  9.64 us
    dot_general x1, matrix products, shards(): lax.dot_general(down_shard, hidden, (((0,), (1,)), ((), ())), preferred_e...  9.25 us
    all_to_all x1, waiting for transfers between devices, shards(): lax.all_to_all(expert_out, 'ep', split_axis=1, concat_axis=1, tiled=True)  7.26 us
    dot_general x1, matrix products, shards(): jnp.dot(picked_rows, expert_gate[0], preferred_element_type=jnp.float32)  4.76 us
  transfers between devices with their start and end apart: 3, of which 3 were waited for; matrix products, arithmetic and copies ran while one was open for 0% of the time, Pallas kernels for 0%

commit v1 on v0

--- a/solution.py
+++ b/solution.py
@@ -7,6 +7,27 @@
 
 
 def shards(tokens, pre_gain, out_gain, chosen, route_weight, expert_gate, expert_up, expert_down):
+
+    def _change_waves(raw):
+        low, kept_arr, built = (jax.lax.axis_size("tp"), jax.lax.axis_index("tp"), raw.shape[1])
+        all_rows = [(i, (i + 1) % low) for i in range(low)]
+        pieces_in = [(i, (i - 1) % low) for i in range(low)]
+        val2 = jnp.zeros((*raw.shape[:1], low * built, *raw.shape[2:]), raw.dtype)
+        val2 = lax.dynamic_update_slice_in_dim(val2, raw, kept_arr * built, axis=1)
+        outcome_arr = right_arr = raw
+        d_next = low // 2
+        for h in range(1, d_next + 1):
+            outcome_arr = jax.lax.ppermute(outcome_arr, "tp", all_rows)
+            val2 = lax.dynamic_update_slice_in_dim(
+                val2, outcome_arr, (kept_arr - h) % low * built, axis=1
+            )
+            if h < low - d_next:
+                right_arr = jax.lax.ppermute(right_arr, "tp", pieces_in)
+                val2 = lax.dynamic_update_slice_in_dim(
+                    val2, right_arr, (kept_arr + h) % low * built, axis=1
+                )
+        return val2
+
     model_width = pre_gain.shape[0]
     shard_width = tokens.shape[1]
     tok_count = tokens.shape[0]
@@ -22,7 +43,7 @@
     normed = (resident * row_scale * gain_slice).astype(jnp.bfloat16)
     outgoing = jnp.take(normed, chosen_here, axis=0)
     incoming = lax.all_to_all(outgoing, "ep", split_axis=0, concat_axis=0, tiled=True)
-    picked_rows = lax.all_gather(incoming.reshape(-1, shard_width), "tp", axis=1, tiled=True)
+    picked_rows = _change_waves(incoming.reshape(-1, shard_width))
     gate_act = jnp.dot(picked_rows, expert_gate[0], preferred_element_type=jnp.float32)
     up_act = jnp.dot(picked_rows, expert_up[0], preferred_element_type=jnp.float32)
     hidden = (jax.nn.silu(gate_act) * up_act).astype(jnp.bfloat16)

time: 151 us -> 144 us (0.954)
  waiting for transfers between devices: 76.1 us -> 65.5 us
  starting transfers between devices: 3.5 us -> 7.29 us
    all_gather x1 -> x0, waiting for transfers between devices: 34.4 us -> none  [shards(): lax.all_gather(incoming.reshape(-1, shard_width), 'tp', axis=1, tiled=True)]
    ppermute x0 -> x3, waiting for transfers between devices: none -> 25.1 us  [the longest x2 20.2 us: _change_waves(): outcome_arr = jax.lax.ppermute(outcome_arr, 'tp', all_rows)]
    ppermute x0 -> x3, starting transfers between devices: none -> 3.83 us  [the longest x1 3.82 us: _change_waves(): right_arr = jax.lax.ppermute(right_arr, 'tp', pieces_in)]
  transfers between devices with their start and end apart: 3 -> 5, of which waited for: 3 -> 5; matrix products, arithmetic and copies ran while one was open for 0% -> 0% of each run, Pallas kernels for 0% -> 0%
where the time goes in v1:
time: 144 us; the launch traced here: 143 us
  waiting for transfers between devices  65.5 us (45%)
  blocking collectives  33.1 us (23%)
  between operations  13.5 us (9%)
  matrix products  13.4 us (9%)
  other arithmetic  8.29 us (6%)
  starting transfers between devices  7.29 us (5%)
  local copies, waits for them, and re-layouts  2.2 us (2%)
    reduce_scatter x1, waiting for transfers between devices, shards(): lax.psum_scatter(lax.dot_general(down_shard, hidden, (((0,), (1,)), ((),...  33.1 us
    ppermute x2, waiting for transfers between devices, _change_waves(): outcome_arr = jax.lax.ppermute(outcome_arr, 'tp', all_rows)  20.2 us
    psum x1, blocking collectives, shards(): square_sum = lax.psum(jnp.sum(resident * resident, axis=1), 'tp')  13.5 us
    all_to_all x1, blocking collectives, shards(): lax.all_to_all(outgoing, 'ep', split_axis=0, concat_axis=0, tiled=True)  10 us
    psum x1, blocking collectives, shards(): out_sum = lax.psum(jnp.sum(mixed_rows * mixed_rows, axis=1), 'tp')  9.64 us
    dot_general x1, matrix products, shards(): lax.dot_general(down_shard, hidden, (((0,), (1,)), ((), ())), preferred_e...  9.26 us
    all_to_all x1, waiting for transfers between devices, shards(): lax.all_to_all(expert_out, 'ep', split_axis=1, concat_axis=1, tiled=True)  7.26 us
    ppermute x1, waiting for transfers between devices, _change_waves(): right_arr = jax.lax.ppermute(right_arr, 'tp', pieces_in)  4.87 us
  transfers between devices with their start and end apart: 5, of which 5 were waited for; matrix products, arithmetic and copies ran while one was open for 0% of the time, Pallas kernels for 0%

profile of v1, /device:TPU:0, one launch (start us, length us, event | category | flops | bytes accessed | tf_op | source)
XLA Modules:
  0.0 143.3 jit_solution(15904103290121605581)
XLA Ops:
  6.5 0.0 reduce-scatter.2.cloned.1.call-start
  6.5 0.7 compare_select_fusion.1
  7.2 0.7 compare_and_fusion
  7.9 1.4 fusion.12
  9.3 13.5 %psum.14 = f32[384]{0:T(512)S(1)} all-reduce(f32[384]{0:T(512)S(1)} %fusion.12), channel_id=1, replica_groups=mesh['grp'=2,'ep'=4,'tp'=4] {'tp'}, use_global_device_ids=true, to_apply=%region_1.0 | all-reduce | flops 384 | bytes 3072 | tf_op jit(solution)/shard_map/psum | solution.py:38
  22.8 0.1 reshape.80
  22.9 0.7 dynamic_slice.3
  23.6 1.4 fusion.14
  24.9 1.0 gather_fusion
  26.0 0.1 broadcast_select_fusion
  26.1 10.0 %all_to_all.10 = bf16[4,48,1024]{2,1,0:T(8,128)(2,1)S(1)} all-to-all(bf16[4,48,1024]{2,1,0:T(8,128)(2,1)S(1)} %broadcast_select_fusion), channel_id=1, replica_groups=mesh['grp'=2,'ep'=4,'tp'=4] {'ep'}, dimensions={0} | all-to-all | bytes 786432 | tf_op jit(solution)/shard_map/all_to_all | solution.py:45
  36.1 0.0 collective-permute-start
  36.1 3.8 %collective-permute-start.1 = (bf16[192,1024]{1,0:T(8,128)(2,1)S(1)}, bf16[192,1024]{1,0:T(8,128)(2,1)S(1)}, u32[]{:S(2)}, u32[]{:S(2)}) collective-permute-start(bf16[192,1024]{1,0:T(8,128)(2,1)S(1)} %bitcast.45), channel_id=1, source_target_pairs={{0,3},{1,0},{2,1},{3,2},{4,7},{5,4},{6,5},{7,6},{8,11},{9,8},{10,9... | collective-permute-start | bytes 1179656 | tf_op jit(solution)/shard_map/ppermute | solution.py:25
  39.9 10.0 %collective-permute-done = bf16[192,1024]{1,0:T(8,128)(2,1)S(1)} collective-permute-done((bf16[192,1024]{1,0:T(8,128)(2,1)S(1)}, bf16[192,1024]{1,0:T(8,128)(2,1)S(1)}, u32[]{:S(2)}, u32[]{:S(2)}) %collective-permute-start) | collective-permute-done | bytes 393248 | tf_op jit(solution)/shard_map/ppermute | solution.py:20
  49.8 0.0 collective-permute-start.2
  49.9 0.2 broadcast_in_dim.22
  50.1 4.9 %collective-permute-done.1 = bf16[192,1024]{1,0:T(8,128)(2,1)S(1)} collective-permute-done((bf16[192,1024]{1,0:T(8,128)(2,1)S(1)}, bf16[192,1024]{1,0:T(8,128)(2,1)S(1)}, u32[]{:S(2)}, u32[]{:S(2)}) %collective-permute-start.1) | collective-permute-done | bytes 393248 | tf_op jit(solution)/shard_map/ppermute | solution.py:25
  55.0 10.2 %collective-permute-done.2 = bf16[192,1024]{1,0:T(8,128)(2,1)S(1)} collective-permute-done((bf16[192,1024]{1,0:T(8,128)(2,1)S(1)}, bf16[192,1024]{1,0:T(8,128)(2,1)S(1)}, u32[]{:S(2)}, u32[]{:S(2)}) %collective-permute-start.2) | collective-permute-done | bytes 393248 | tf_op jit(solution)/shard_map/ppermute | solution.py:20
  65.3 4.2 %fusion.2 = f32[192,768]{1,0:T(8,128)S(1)} fusion(bf16[192,4096]{1,0:T(8,128)(2,1)S(1)} %constant_dynamic-update-slice_fusion, bf16[1,4096,768]{2,1,0:T(8,128)(2,1)} %param.14), kind=kOutput, calls=%fused_computation.4 | convolution fusion | flops 1207959552 | bytes 8454144 | tf_op jit(solution)/shard_map/dot_general | solution.py:48
  69.5 9.3 %fusion.9 = bf16[4096,192]{0,1:T(8,128)(2,1)} fusion(bf16[1,768,4096]{2,1,0:T(8,128)(2,1)} %param.15, f32[192,768]{1,0:T(8,128)S(1)} %fusion.2, bf16[192,4096]{1,0:T(8,128)(2,1)S(1)} %constant_dynamic-update-slice_fusion, bf16[1,4096,768]{2,1,0:T(8,128)(2,1)} %param.13), kind=kOutput, calls=%fused_computation.9 | convolution fusion | flops 2417590272 | bytes 16318464 | tf_op jit(solution)/shard_map/dot_general | solution.py:52
  78.7 0.0 copy-start.1
  78.7 0.0 copy-start.3
  78.7 0.0 reduce-scatter.2.cloned.1.call-update
  78.8 33.1 %reduce-scatter.2.cloned.1.call-done = bf16[1024,192]{0,1:T(8,128)(2,1)} async-done(((bf16[4096,192]{0,1:T(8,128)(2,1)}), bf16[1024,192]{0,1:T(8,128)(2,1)}) %reduce-scatter.2.cloned.1.call-update) | async-done | bytes 393232 | tf_op jit(solution)/shard_map/reduce_scatter | solution.py:51
  111.9 3.5 %all-to-all-start.1 = ((bf16[1024,4,48]{0,2,1:T(8,128)(2,1)}), bf16[1024,4,48]{0,2,1:T(8,128)(2,1)S(1)}, u32[]{:S(2)}, u32[]{:S(2)}) async-start(bf16[1024,4,48]{0,2,1:T(8,128)(2,1)} %bitcast.48), calls=%async_computation.2 | async-start | bytes 786432 | tf_op jit(solution)/shard_map/all_to_all | solution.py:60
  115.4 0.0 copy-done.1
  115.4 0.0 copy-start
  115.4 0.1 reshape_squeeze.3
  115.5 7.3 %all-to-all-done.1 = bf16[1024,4,48]{0,2,1:T(8,128)(2,1)S(1)} async-done(((bf16[1024,4,48]{0,2,1:T(8,128)(2,1)}), bf16[1024,4,48]{0,2,1:T(8,128)(2,1)S(1)}, u32[]{:S(2)}, u32[]{:S(2)}) %all-to-all-start.1) | async-done | bytes 393248 | tf_op jit(solution)/shard_map/all_to_all | solution.py:60
  122.7 0.0 copy-done.3
  122.7 0.1 convert_multiply_fusion.2
  122.9 2.5 %scatter_custom_fusion = f32[1024,384]{0,1:T(8,128)S(1)} fusion(s32[192]{0:T(256)S(1)} %bitcast.50, f32[192,1024]{1,0:T(8,128)S(1)} %bitcast.47, f32[]{:T(128)} %constant.51.clone.1), kind=kCustom, calls=%fused_computation.19 | custom fusion | flops 196608 | bytes 1572868 | tf_op jit(solution)/shard_map/scatter-add | solution.py:66
  125.4 0.0 copy-done
  125.4 0.0 copy-start.2
  125.4 0.3 multiply_reduce_fusion
  125.7 9.6 %psum.15 = f32[384]{0:T(512)S(1)} all-reduce(f32[384]{0:T(512)S(1)} %multiply_reduce_fusion), channel_id=1, replica_groups=mesh['grp'=2,'ep'=4,'tp'=4] {'tp'}, use_global_device_ids=true, to_apply=%region_5.6 | all-reduce | flops 384 | bytes 3072 | tf_op jit(solution)/shard_map/psum | solution.py:69
  135.3 0.0 copy-done.2
  135.3 1.1 multiply_convert_fusion
  (8 shorter events, 0.2 us)
Async XLA Ops:
  6.5 105.4 %reduce-scatter.2.cloned.1.call-start = ((), (), s32[]{:S(2)}) async-start(), calls=%async_computation.3 | async-start | bytes 1966080 | tf_op jit(solution)/shard_map/reduce_scatter | solution.py:51
  36.1 13.8 %collective-permute-start = (bf16[192,1024]{1,0:T(8,128)(2,1)S(1)}, bf16[192,1024]{1,0:T(8,128)(2,1)S(1)}, u32[]{:S(2)}, u32[]{:S(2)}) collective-permute-start(bf16[192,1024]{1,0:T(8,128)(2,1)S(1)} %bitcast.44), channel_id=1, source_target_pairs={{0,1},{1,2},{2,3},{3,0},{4,5},{5,6},{6,7},{7,4},{8,9},{9,10},{10,1... | collective-permute-start | bytes 1179656 | tf_op jit(solution)/shard_map/ppermute | solution.py:20
  36.1 18.9 %collective-permute-start.1 = (bf16[192,1024]{1,0:T(8,128)(2,1)S(1)}, bf16[192,1024]{1,0:T(8,128)(2,1)S(1)}, u32[]{:S(2)}, u32[]{:S(2)}) collective-permute-start(bf16[192,1024]{1,0:T(8,128)(2,1)S(1)} %bitcast.45), channel_id=1, source_target_pairs={{0,3},{1,0},{2,1},{3,2},{4,7},{5,4},{6,5},{7,6},{8,11},{9,8},{10,9... | collective-permute-start | bytes 1179656 | tf_op jit(solution)/shard_map/ppermute | solution.py:25
  49.8 15.4 %collective-permute-start.2 = (bf16[192,1024]{1,0:T(8,128)(2,1)S(1)}, bf16[192,1024]{1,0:T(8,128)(2,1)S(1)}, u32[]{:S(2)}, u32[]{:S(2)}) collective-permute-start(bf16[192,1024]{1,0:T(8,128)(2,1)S(1)} %collective-permute-done), channel_id=1, source_target_pairs={{0,1},{1,2},{2,3},{3,0},{4,5},{5,6},{6,7},{7,4},{8,9},{9,10},{10,1... | collective-permute-start | bytes 1179656 | tf_op jit(solution)/shard_map/ppermute | solution.py:20
  78.7 36.6 %copy-start.1 = (s32[1,4,48]{2,1,0:T(4,128)S(1)}, s32[1,4,48]{2,1,0:T(4,128)}, u32[]{:S(2)}) copy-start(s32[1,4,48]{2,1,0:T(4,128)} %param.11) | copy-start | bytes 2308
  78.7 44.0 %copy-start.3 = (f32[1,4,48]{2,1,0:T(4,128)S(1)}, f32[1,4,48]{2,1,0:T(4,128)}, u32[]{:S(2)}) copy-start(f32[1,4,48]{2,1,0:T(4,128)} %param.12) | copy-start | bytes 2308
  111.9 10.8 %all-to-all-start.1 = ((bf16[1024,4,48]{0,2,1:T(8,128)(2,1)}), bf16[1024,4,48]{0,2,1:T(8,128)(2,1)S(1)}, u32[]{:S(2)}, u32[]{:S(2)}) async-start(bf16[1024,4,48]{0,2,1:T(8,128)(2,1)} %bitcast.48), calls=%async_computation.2 | async-start | bytes 786432 | tf_op jit(solution)/shard_map/all_to_all | solution.py:60
  115.4 10.0 %copy-start = (bf16[384,1024]{1,0:T(8,128)(2,1)S(1)}, bf16[384,1024]{1,0:T(8,128)(2,1)}, u32[]{:S(2)}) copy-start(bf16[384,1024]{1,0:T(8,128)(2,1)} %param.8) | copy-start | bytes 2359300
  125.4 9.9 %copy-start.2 = (f32[1024]{0:T(1024)S(1)}, f32[1024]{0:T(1024)}, u32[]{:S(2)}) copy-start(f32[1024]{0:T(1024)} %param.10) | copy-start | bytes 12292
Sparse Core Ops, SparseCore 0:
  78.9 32.9 reduce-scatter.1
